TPU v7x, 32 devices: a whole 2x2x4 slice. The times are simulated.
32 devices in a mesh: ep: 4 (over y, x), tp: 8 (over z, core).
Axes of the slice: x: 2, y: 2, z: 4, core: 2. Of those that a mesh axis runs over, the one named last changes fastest.
Arguments:
- mix_in: bfloat16 [4096, 2048], P(('ep', 'tp')), may hold values from -6 to 6
- mix_gain: float32 [2048], replicated, may hold values from 0.1 to 1.9
- mix_w_in: bfloat16 [2048, 512], P('tp'), may hold values from -0.125 to 0.125
- pool_mat: bfloat16 [4, 128, 128], replicated, may hold values from -0.5 to 0.5
- pool_scale: float32 [512], replicated, may hold values from 0.1 to 1.9
- mix_w_out: bfloat16 [512, 2048], P(None, 'tp'), may hold values from -0.25 to 0.25
- moe_in: bfloat16 [4096, 2048], P(('ep', 'tp')), may hold values from -6 to 6
- moe_gain: float32 [2048], replicated, may hold values from 0.1 to 1.9
- routes: int32 [4096, 2], P('ep'), may hold values from 0 to 31, all different within a row; in each aligned block of 1024 rows (0 to 1023, 1024 to 2047, ...) at most 128 rows name the same one
- route_score: bfloat16 [4096, 2], P('ep'), may hold values from 0.099609375 to 1
- exp_gate: bfloat16 [32, 2048, 768], P(('ep', 'tp')), may hold values from -0.125 to 0.125
- exp_up: bfloat16 [32, 2048, 768], P(('ep', 'tp')), may hold values from -0.125 to 0.125
- exp_down: bfloat16 [32, 768, 2048], P(('ep', 'tp')), may hold values from -0.21875 to 0.21875
- shared_gate: bfloat16 [768, 2048], P('tp'), may hold values from -0.125 to 0.125
- shared_up: bfloat16 [768, 2048], P('tp'), may hold values from -0.125 to 0.125
- shared_down: bfloat16 [768, 2048], P('tp'), may hold values from -0.21875 to 0.21875
Outputs:
- mixed: bfloat16 [4096, 2048], P(('ep', 'tp'))
- moe_out: bfloat16 [4096, 2048], P(('ep', 'tp'))
Inputs may be any that keep to these rules, and one draw needn't show every extreme that they name: `routes`: each row names 2 different experts. Within the rows of one index of ep (aligned blocks of 1024 rows) no expert is named more than 128 times, a bound that some expert reaches in some blocks.
All inputs are finite; a program needn't handle non-finite values.
Results may differ from a plain program's by a relative error of at most 0.012.
Values may be sent and summed in bfloat16 or wider, within the bound.
A program may use at most 128 MiB of HBM per device.

v0:
```python
import functools

import jax
import jax.numpy as jnp
from jax import lax
from jax.experimental import pallas as pl
from jax.experimental.pallas import tpu as pltpu
from jax.sharding import PartitionSpec as P

SEQS_MIX = 1
CORES = 2

NORM_EPS = 1e-06
ROUTED_SCALE = 2.5
MESH = pl.DeviceIdType.MESH


def rms_rows(values, gain):
    floats = values.astype(jnp.float32)
    scaled = floats * lax.rsqrt(jnp.mean(floats * floats, axis=-1, keepdims=True) + NORM_EPS)
    return (scaled * gain).astype(jnp.bfloat16)


def remote(src, dst, send_sem, recv_sem, device):
    return pltpu.make_async_remote_copy(
        src_ref=src,
        dst_ref=dst,
        send_sem=send_sem,
        recv_sem=recv_sem,
        device_id=device,
        device_id_type=MESH,
    )


def greet(devices):
    barrier = pltpu.get_barrier_semaphore()
    for device in devices:
        pl.semaphore_signal(barrier, inc=1, device_id=device, device_id_type=MESH)
    pl.semaphore_wait(barrier, len(devices))


class Place:
    def __init__(self, ep_count, tp_count):
        self.ep_count, self.tp_count = ep_count, tp_count
        self.chips = tp_count // CORES
        self.far = self.chips // 2
        self.ep, self.tp = lax.axis_index("ep"), lax.axis_index("tp")
        self.chip, self.core = self.tp // CORES, self.tp % CORES

    def at(self, step):
        return (self.chip + step + self.chips) % self.chips

    def column(self, step, core):
        return self.at(step) * CORES + core

    def side(self, way):
        return (self.ep, self.column(1 if way == 0 else -1, self.core))

    def sibling(self):
        return (self.ep, self.column(0, 1 - self.core))

    def peers(self):
        return [((self.ep + i) % self.ep_count, self.tp) for i in range(1, self.ep_count)]


def ring_keys(chips):
    far = chips // 2
    return [
        (way, dist, half)
        for dist in range(1, far + 1)
        for turn in range(2)
        for way, half in ((0, turn), (1, 1 - turn))
        if dist < far or half == way
    ]


class RingGather:
    def __init__(self, place, buf, send, recv):
        self.place, self.buf, self.send, self.recv = place, buf, send, recv
        self.rows = buf.shape[1] // 2
        self.keys = ring_keys(place.chips)
        self.started = []

    def view(self, step, core, half):
        return self.buf.at[self.place.column(step, core), pl.ds(half * self.rows, self.rows)]

    def push(self, key):
        way, dist, half = key
        n = self.keys.index(key)
        block = self.view(-(dist - 1) if way == 0 else dist - 1, self.place.core, half)
        self._go(block, n, self.place.side(way))

    def _go(self, block, n, device):
        copy = remote(block, block, self.send.at[n], self.recv.at[n], device)
        copy.start()
        self.started.append(copy)

    def _arrived(self, block, n, device):
        remote(block, block, self.send.at[n], self.recv.at[n], device).wait_recv()

    def start(self):
        for key in self.keys:
            if key[1] == 1:
                self.push(key)
        block = self.buf.at[self.place.tp]
        self._go(block, 2 * len(self.keys), self.place.sibling())

    def step(self, dist):
        for n, key in enumerate(self.keys):
            if key[1] != dist:
                continue
            way, _, half = key
            block = self.view(-dist if way == 0 else dist, self.place.core, half)
            self._arrived(block, n, self.place.side(way))
            if (way, dist + 1, half) in self.keys:
                self.push((way, dist + 1, half))
            self._go(block, len(self.keys) + n, self.place.sibling())

    def arrive(self):
        for n, (way, dist, half) in enumerate(self.keys):
            block = self.view(-dist if way == 0 else dist, 1 - self.place.core, half)
            self._arrived(block, len(self.keys) + n, self.place.sibling())
        block = self.buf.at[self.place.column(0, 1 - self.place.core)]
        self._arrived(block, 2 * len(self.keys), self.place.sibling())

    def close(self):
        for copy in self.started:
            copy.wait_send()


def layer_kernel(
    ep_count, tp_count, seq_len,
    moe_in, moe_gain, routes, scores, shared_gate, shared_up, shared_down, mix_w_in, mix_w_out,
    mix_in, mix_gain, pool_mat, pool_scale, exp_gate, exp_up, exp_down,
    mixed, moe_out,
    tokens, outgoing, received, results, returned, pick, share, total, w_in, w_out,
    gate_w, up_w, down_w, gate_sum, up_sum, from_sibling, sums, arrived, tail, prior,
    ws, xs, xr, ins, inr, outs, outr, as_, ar, bs, br, hs, hr, ss, sr, rs, rr,
):
    place = Place(ep_count, tp_count)
    devices = ep_count * tp_count
    flat = place.ep * tp_count + place.tp
    after, before = (flat + 1) % devices, (flat + devices - 1) % devices
    after = (after // tp_count, after % tp_count)
    before = (before // tp_count, before % tp_count)
    loads = [
        pltpu.make_async_copy(src.at[0], dst, ws.at[n])
        for n, (src, dst) in enumerate(((exp_gate, gate_w), (exp_up, up_w), (exp_down, down_w)))
    ]
    for load in loads:
        load.start()
    greet([place.side(0), place.side(1), place.sibling(), after, before] + place.peers())
    me = place.tp
    rows, width = moe_in.shape
    pieces, cut = tokens.shape[0], tokens.shape[3]
    capacity = outgoing.shape[2]
    slots = ep_count * capacity
    block_rows = tp_count * rows
    far = place.far
    sent = []

    normed = rms_rows(moe_in[...], moe_gain[...])
    for c in range(pieces):
        tokens[c, pl.ds(me, 1)] = normed[:, c * cut : (c + 1) * cut][None]
    gathers = [RingGather(place, tokens.at[c], xs.at[c], xr.at[c]) for c in range(pieces)]
    gathers[0].start()
    gathers[1].start()

    top_count = routes.shape[0]
    lines = max(8, ep_count)
    names = lax.broadcasted_iota(jnp.int32, (lines, block_rows), 0) * tp_count + me
    score_sum = jnp.sum(scores[...], axis=0, keepdims=True)
    named = jnp.zeros((lines, block_rows), jnp.float32)
    weight = jnp.zeros((lines, block_rows), jnp.float32)
    for k in range(top_count):
        hit = routes[k : k + 1, :] == names
        named = named + jnp.where(hit, 1.0, 0.0)
        weight = weight + jnp.where(hit, scores[k : k + 1, :] / score_sum * ROUTED_SCALE, 0.0)
    ones = named.astype(jnp.bfloat16)
    earlier = []
    for low in range(0, block_rows, 512):
        source = lax.broadcasted_iota(jnp.int32, (block_rows, 512), 0)
        target = lax.broadcasted_iota(jnp.int32, (block_rows, 512), 1) + low
        strict = jnp.where(source < target, 1.0, 0.0).astype(jnp.bfloat16)
        earlier.append(jnp.dot(ones, strict, preferred_element_type=jnp.float32))
    spot = jnp.where(named > 0.5, jnp.concatenate(earlier, axis=1), -1.0).astype(jnp.int32)
    slot = lax.broadcasted_iota(jnp.int32, (capacity, block_rows), 0)
    for j in range(ep_count):
        here = spot[j : j + 1, :] == slot
        span = slice(j * capacity, (j + 1) * capacity)
        pick[span, :] = jnp.where(here, 1.0, 0.0).astype(jnp.bfloat16)
        weighed = jnp.where(here, weight[j : j + 1, :], 0.0).T.astype(jnp.bfloat16)
        share[:, :, span] = weighed.reshape(tp_count, rows, capacity)

    def scatter(source, landing, c, send, recv):
        for i, (peer, column) in enumerate(place.peers()):
            copy = remote(
                source.at[c, peer], landing.at[c, place.ep], send.at[c, i], recv.at[c, i],
                (peer, column),
            )
            copy.start()
            sent.append(copy)
        landing[c, pl.ds(place.ep, 1)] = source[c, pl.ds(place.ep, 1)]

    def landing_wait(landing, c, send, recv):
        for i in range(1, ep_count):
            peer = (place.ep - i + ep_count) % ep_count
            block = landing.at[c, peer]
            remote(block, block, send.at[c, i - 1], recv.at[c, i - 1], (peer, me)).wait_recv()

    for c in range(pieces):
        for dist in range(1, far + 1):
            gathers[c].step(dist)
            if dist == 1 and c + 2 < pieces:
                gathers[c + 2].start()
        gathers[c].arrive()
        picked = jnp.dot(
            pick[...], tokens[c].reshape(block_rows, cut), preferred_element_type=jnp.float32
        )
        outgoing[c] = picked.astype(jnp.bfloat16).reshape(ep_count, capacity, cut)
        scatter(outgoing, received, c, as_, ar)

    w_in[pl.ds(me, 1)] = mix_w_in[...][None]
    w_out[pl.ds(me, 1)] = mix_w_out[...][None]
    first = RingGather(place, w_in, ins, inr)
    second = RingGather(place, w_out, outs, outr)
    first.start()
    second.start()

    def ffn(i, carry):
        across = (((1,), (1,)), ((), ()))
        pair = pl.ds(i * CORES, CORES)
        gate = jnp.zeros((CORES * rows, shared_gate.shape[0]), jnp.float32)
        up = gate
        for c in range(pieces):
            block = tokens[c, pair].reshape(CORES * rows, cut)
            span = slice(c * cut, (c + 1) * cut)
            gate = gate + lax.dot_general(
                block, shared_gate[:, span], across, preferred_element_type=jnp.float32
            )
            up = up + lax.dot_general(
                block, shared_up[:, span], across, preferred_element_type=jnp.float32
            )
        hidden = (jax.nn.silu(gate) * up).astype(jnp.bfloat16)
        for c in range(pieces):
            value = jnp.dot(
                hidden, shared_down[:, c * cut : (c + 1) * cut], preferred_element_type=jnp.float32
            )
            total[c, pair] = value.astype(jnp.bfloat16).reshape(CORES, rows, cut)
        return carry

    lax.fori_loop(0, tp_count // CORES, ffn, 0)

    for load in loads:
        load.wait()
    for c in range(pieces):
        landing_wait(received, c, as_, ar)
        block = received[c].reshape(slots, cut)
        for acc, weights in ((gate_sum, gate_w), (up_sum, up_w)):
            value = jnp.dot(
                block, weights[c * cut : (c + 1) * cut, :], preferred_element_type=jnp.float32
            )
            acc[...] = value if c == 0 else acc[...] + value
    hidden = (jax.nn.silu(gate_sum[...]) * up_sum[...]).astype(jnp.bfloat16)
    for c in range(pieces):
        value = jnp.dot(
            hidden, down_w[:, c * cut : (c + 1) * cut], preferred_element_type=jnp.float32
        )
        results[c] = value.astype(jnp.bfloat16).reshape(ep_count, capacity, cut)
        scatter(results, returned, c, bs, br)

    for dist in range(1, far + 1):
        first.step(dist)
        second.step(dist)

    order = [far]
    for dist in range(far - 1, 0, -1):
        order += [dist, -dist]
    order += [0]
    half_rows = rows // 2
    keys = ring_keys(place.chips)

    def halves(half):
        return pl.ds(half * half_rows, half_rows)

    def landed(c, key):
        n = keys.index(key)
        block = arrived.at[c, n]
        remote(block, block, rs.at[c, n], rr.at[c, n], place.side(key[0])).wait_recv()
        return arrived[c, n].astype(jnp.float32)

    def chip_sum(c, chip, half):
        mine = total[c, pl.ds(chip * CORES + place.core, 1), halves(half)]
        theirs = from_sibling[c, pl.ds(chip, 1), halves(half)]
        return (mine.astype(jnp.float32) + theirs.astype(jnp.float32))[0]

    def sibling_wait(c, n):
        block = from_sibling.at[c, place.at(order[n])]
        remote(block, block, ss.at[c, n], sr.at[c, n], place.sibling()).wait_recv()

    def pass_on(c, n):
        step = order[n]
        dist = abs(step)
        sibling_wait(c, n)
        ways = (0, 1) if dist == far else ((0,) if step > 0 else (1,))
        for k, (way, d, half) in enumerate(keys):
            if d != dist or way not in ways:
                continue
            value = chip_sum(c, place.at(step), half)
            if (way, dist + 1, half) in keys:
                value = value + landed(c, (way, dist + 1, half))
            sums[c, k] = value.astype(jnp.bfloat16)
            copy = remote(
                sums.at[c, k], arrived.at[c, k], rs.at[c, k], rr.at[c, k], place.side(way)
            )
            copy.start()
            sent.append(copy)

    for c in range(pieces):
        landing_wait(returned, c, bs, br)
        for n, step in enumerate(order):
            chip = place.at(step)
            pair = pl.ds(chip * CORES, CORES)
            value = jnp.dot(
                share[pair].reshape(CORES * rows, slots),
                returned[c].reshape(slots, cut),
                preferred_element_type=jnp.float32,
            ).reshape(CORES, rows, cut)
            total[c, pair] = (value + total[c, pair].astype(jnp.float32)).astype(jnp.bfloat16)
            copy = remote(
                total.at[c, chip * CORES + 1 - place.core], from_sibling.at[c, chip],
                ss.at[c, n], sr.at[c, n], place.sibling(),
            )
            copy.start()
            sent.append(copy)
        pass_on(c, 0)

    first.arrive()
    second.arrive()
    groups, group_ch = pool_mat.shape[0], pool_mat.shape[1]
    reach = 2**groups
    mix_normed = rms_rows(mix_in[...], mix_gain[...])
    projected = jnp.dot(
        mix_normed, w_in[...].reshape(width, groups * group_ch), preferred_element_type=jnp.float32
    ).astype(jnp.bfloat16)
    tail[...] = projected[rows - reach :]
    halo = remote(tail, prior, hs, hr, after)
    halo.start()
    for n in range(1, len(order) - 1):
        for c in range(pieces):
            pass_on(c, n)
    halo.wait()
    first_row = flat * rows
    keep = jnp.where(first_row % seq_len == 0, 0.0, 1.0)
    extended = jnp.concatenate(
        [prior[...].astype(jnp.float32) * keep, projected.astype(jnp.float32)], axis=0
    )
    position = (first_row + lax.broadcasted_iota(jnp.int32, (rows, group_ch), 0)) % seq_len
    pooled_parts = []
    for group in range(groups):
        channels = slice(group * group_ch, (group + 1) * group_ch)
        running = extended[:, channels]
        for level in range(group + 1):
            running = running + pltpu.roll(running, 2**level, 0)
        counts = jnp.minimum(position + 1, 2 ** (group + 1)).astype(jnp.float32)
        pooled = (running[reach:] / counts - extended[reach:, channels]).astype(jnp.bfloat16)
        grouped = jnp.dot(pooled, pool_mat[group], preferred_element_type=jnp.float32)
        pooled_parts.append((grouped * pool_scale[:, channels]).astype(jnp.bfloat16))
    pool_out = jnp.concatenate(pooled_parts, axis=1)
    span = w_out.shape[2]
    for column in range(tp_count):
        mixed[:, column * span : (column + 1) * span] = jnp.dot(
            pool_out, w_out[column], preferred_element_type=jnp.float32
        ).astype(jnp.bfloat16)

    for c in range(pieces):
        sibling_wait(c, len(order) - 1)
        for half in range(2):
            value = chip_sum(c, place.chip, half)
            for way in range(2):
                if (way, 1, half) in keys:
                    value = value + landed(c, (way, 1, half))
            moe_out[half * half_rows : (half + 1) * half_rows, c * cut : (c + 1) * cut] = (
                value.astype(jnp.bfloat16)
            )
    for copy in sent:
        copy.wait_send()
    for gather in gathers + [first, second]:
        gather.close()


def vmem(count):
    return [pl.BlockSpec(memory_space=pltpu.VMEM)] * count


def shards(
    mix_in, mix_gain, mix_w_in, pool_mat, pool_scale, mix_w_out, moe_in, moe_gain, routes,
    route_score, exp_gate, exp_up, exp_down, shared_gate, shared_up, shared_down,
):
    ep_count, tp_count = lax.axis_size("ep"), lax.axis_size("tp")
    rows, width = moe_in.shape
    block_rows, top_count = routes.shape
    capacity = 2 * block_rows * top_count // (ep_count * tp_count)
    slots = ep_count * capacity
    dma = lambda n: pltpu.SemaphoreType.DMA((n,))
    bf16 = jnp.bfloat16
    messages = len(ring_keys(tp_count // CORES))

    chips = tp_count // CORES
    pieces = 4
    cut = width // pieces
    hidden = exp_gate.shape[2]
    reach = 2 ** pool_mat.shape[0]
    seq_len = mix_in.shape[0] * ep_count * tp_count // SEQS_MIX
    grid = lambda n: pltpu.SemaphoreType.DMA((pieces, n))
    buffer = lambda *shape: pltpu.VMEM(shape, bf16)
    mixed, moe_out = pl.pallas_call(
        functools.partial(layer_kernel, ep_count, tp_count, seq_len),
        out_shape=[
            jax.ShapeDtypeStruct(mix_in.shape, bf16),
            jax.ShapeDtypeStruct(moe_in.shape, bf16),
        ],
        in_specs=vmem(13) + [pl.BlockSpec(memory_space=pl.ANY)] * 3,
        out_specs=vmem(2),
        scratch_shapes=[
            buffer(pieces, tp_count, rows, cut),
            buffer(pieces, ep_count, capacity, cut),
            buffer(pieces, ep_count, capacity, cut),
            buffer(pieces, ep_count, capacity, cut),
            buffer(pieces, ep_count, capacity, cut),
            buffer(slots, block_rows),
            buffer(tp_count, rows, slots),
            buffer(pieces, tp_count, rows, cut),
            buffer(tp_count, *mix_w_in.shape),
            buffer(tp_count, *mix_w_out.shape),
            buffer(width, hidden),
            buffer(width, hidden),
            buffer(hidden, width),
            pltpu.VMEM((slots, hidden), jnp.float32),
            pltpu.VMEM((slots, hidden), jnp.float32),
            buffer(pieces, chips, rows, cut),
            buffer(pieces, messages, rows // 2, cut),
            buffer(pieces, messages, rows // 2, cut),
            buffer(reach, mix_w_in.shape[1]),
            buffer(reach, mix_w_in.shape[1]),
            dma(3),
            grid(2 * messages + 1),
            grid(2 * messages + 1),
        ]
        + [dma(2 * messages + 1) for _ in range(4)]
        + [grid(ep_count - 1) for _ in range(4)]
        + [pltpu.SemaphoreType.DMA, pltpu.SemaphoreType.DMA]
        + [grid(chips), grid(chips), grid(messages), grid(messages)],
        compiler_params=pltpu.CompilerParams(
            collective_id=0, has_side_effects=True, vmem_limit_bytes=67043328
        ),
    )(
        moe_in, moe_gain[None, :], routes.T, route_score.T.astype(jnp.float32), shared_gate,
        shared_up, shared_down, mix_w_in, mix_w_out, mix_in, mix_gain[None, :], pool_mat,
        pool_scale[None, :], exp_gate, exp_up, exp_down,
    )
    return (mixed, moe_out)


def solution(mesh):
    return jax.shard_map(
        shards,
        mesh=mesh,
        in_specs=(
            P(("ep", "tp"), None),
            P(),
            P("tp", None),
            P(),
            P(),
            P(None, "tp"),
            P(("ep", "tp"), None),
            P(),
            P("ep", None),
            P("ep", None),
            P(("ep", "tp"), None, None),
            P(("ep", "tp"), None, None),
            P(("ep", "tp"), None, None),
            P("tp", None),
            P("tp", None),
            P("tp", None),
        ),
        out_specs=(P(("ep", "tp"), None), P(("ep", "tp"), None)),
        check_vma=False,
    )
```

profile of v0, /device:TPU:0, one launch (start us, length us, event | category | flops | bytes accessed | tf_op | source)
XLA Modules:
  0.0 131.5 jit_solution(12201692519339006460)
XLA Ops:
  0.6 1.3 convert_bitcast_fusion.scores
  1.9 125.8 %shard_map.167 = (bf16[128,2048]{1,0:T(8,128)(2,1)}, bf16[128,2048]{1,0:T(8,128)(2,1)}) custom-call(bf16[128,2048]{1,0:T(8,128)(2,1)} %moe_in.1, f32[1,2048]{1,0:T(1,128)} %bitcast.6, s32[2,1024]{1,0:T(2,128)} %bitcast.7, f32[2,1024]{1,0:T(2,128)} %convert_bitcast_fusion.scores, bf16[96,2048]{1,0:T(8,128)(2,1)} %shared_gate.1, bf16[96,2048]{1,0:T(8,128)(2,1)} %shared_up.1, ...), custom_call_target="tpu_custom_call" | custom-call | tf_op jit(solution)/shard_map/pallas_call | solution.py:417
  127.7 1.9 %copy.20 = bf16[128,2048]{1,0:T(8,128)(2,1)} copy(bf16[128,2048]{1,0:T(8,128)(2,1)} %get-tuple-element.4) | data formatting | bytes 1048576
  129.6 1.9 %copy.21 = bf16[128,2048]{1,0:T(8,128)(2,1)} copy(bf16[128,2048]{1,0:T(8,128)(2,1)} %get-tuple-element.5) | data formatting | bytes 1048576
where the time goes:
time: 132 us; the launch traced here: 131 us
  Pallas kernels  126 us (95%)
  local copies, waits for them, and re-layouts  3.76 us (3%)
    pallas_call x1, Pallas kernels, shards(): pl.pallas_call(functools.partial(layer_kernel, ep_count, tp_count, seq_le...  126 us
    unnamed x2, local copies, waits for them, and re-layouts  3.76 us

commit v1 on v0

v1 whole, which is shorter than its diff:
```python
import functools

import jax
import jax.numpy as jnp
from jax import lax
from jax.experimental import pallas as pl
from jax.experimental.pallas import tpu as pltpu
from jax.sharding import PartitionSpec as P

SEQS_MIX = 1
CORES = 2

NORM_EPS = 1e-06
ROUTED_SCALE = 2.5
MESH = pl.DeviceIdType.MESH
GATHER_CUTS = (4, 4, 4, 4)
RETURN_CUTS = (4, 4, 4, 4)


def rms_rows(values, gain):
    floats = values.astype(jnp.float32)
    scaled = floats * lax.rsqrt(jnp.mean(floats * floats, axis=-1, keepdims=True) + NORM_EPS)
    return (scaled * gain).astype(jnp.bfloat16)


def remote(src, dst, send_sem, recv_sem, device):
    return pltpu.make_async_remote_copy(
        src_ref=src,
        dst_ref=dst,
        send_sem=send_sem,
        recv_sem=recv_sem,
        device_id=device,
        device_id_type=MESH,
    )


def spans_of(width, cuts):
    spans, low = [], 0
    for cut in cuts:
        size = width * cut // sum(cuts)
        spans.append(slice(low, low + size))
        low += size
    return spans


class Place:
    def __init__(self, ep_count, tp_count):
        self.ep_count, self.tp_count = ep_count, tp_count
        self.chips = tp_count // CORES
        self.ep, self.tp = lax.axis_index("ep"), lax.axis_index("tp")
        self.chip, self.core = self.tp // CORES, self.tp % CORES
        self.keys = [(way, d) for d in range(1, self.chips) for way in range(2)]

    def key(self, way, d):
        return self.keys.index((way, d))

    def ahead(self, way):
        return self.chip < self.chips - 1 if way == 0 else self.chip > 0

    def behind(self, way, d):
        return self.chip >= d if way == 0 else self.chip < self.chips - d

    def beyond(self, way, d):
        return self.chip < self.chips - d if way == 0 else self.chip >= d

    def origin(self, way, d):
        return self.chip - d if way == 0 else self.chip + d

    def target(self, way, d):
        return self.chip + d if way == 0 else self.chip - d

    def side(self, way):
        return (self.ep, self.target(way, 1) * CORES + self.core)

    def sibling(self):
        return (self.ep, self.chip * CORES + 1 - self.core)

    def peers(self):
        return [((self.ep + i) % self.ep_count, self.tp) for i in range(1, self.ep_count)]


class LineGather:
    def __init__(self, place, buf, send, recv):
        self.place, self.buf, self.send, self.recv = place, buf, send, recv
        self.count = len(place.keys)

    def block(self, chip, core):
        return self.buf.at[chip, core]

    def push(self, way, d):
        place, n = self.place, self.place.key(way, d)
        block = self.block(place.origin(way, d - 1), place.core)
        return remote(block, block, self.send.at[n], self.recv.at[n], place.side(way))

    def pass_over(self, way, d):
        place, n = self.place, self.count + self.place.key(way, d)
        block = self.block(place.origin(way, d), place.core)
        return remote(block, block, self.send.at[n], self.recv.at[n], place.sibling())

    def own_over(self):
        place, n = self.place, 2 * self.count
        block = self.block(place.chip, place.core)
        return remote(block, block, self.send.at[n], self.recv.at[n], place.sibling())

    def start(self, over=True):
        for way in range(2):
            pl.when(self.place.ahead(way))(lambda way=way: self.push(way, 1).start())
        if over:
            self.own_over().start()

    def step(self, d, onward=True, last=True):
        place = self.place
        for way in range(2):

            def receive(way=way):
                n = place.key(way, d)
                block = self.block(place.origin(way, d), place.core)
                remote(
                    block, block, self.send.at[n], self.recv.at[n], place.sibling()
                ).wait_recv()

            def forward(way=way):
                receive(way)
                if d + 1 < place.chips:
                    self.push(way, d + 1).start()
                self.pass_over(way, d).start()

            def finish(way=way):
                receive(way)
                self.pass_over(way, d).start()

            if onward:
                pl.when(place.behind(way, d) & place.ahead(way))(forward)
            if last:
                pl.when(place.behind(way, d) & jnp.logical_not(place.ahead(way)))(finish)

    def arrive(self):
        place = self.place
        for n, (way, d) in enumerate(place.keys):

            def landed(way=way, d=d, n=n):
                block = self.block(place.origin(way, d), 1 - place.core)
                m = self.count + n
                remote(
                    block, block, self.send.at[m], self.recv.at[m], place.sibling()
                ).wait_recv()

            pl.when(place.behind(way, d))(landed)
        block = self.block(place.chip, 1 - place.core)
        m = 2 * self.count
        remote(block, block, self.send.at[m], self.recv.at[m], place.sibling()).wait_recv()

    def close(self):
        place = self.place
        for way, d in place.keys:
            pl.when(place.behind(way, d - 1) & place.ahead(way))(
                lambda way=way, d=d: self.push(way, d).wait_send()
            )
            pl.when(place.behind(way, d))(
                lambda way=way, d=d: self.pass_over(way, d).wait_send()
            )
        self.own_over().wait_send()


def layer_kernel(
    ep_count, tp_count, seq_len, gather_cuts, return_cuts,
    moe_in, moe_gain, routes, scores, mix_gain, pool_mat, pool_scale,
    shared_gate, shared_up, shared_down, mix_w_in, mix_w_out, mix_in, exp_gate, exp_up, exp_down,
    mixed, moe_out,
    *scratch,
):
    scratch = list(scratch)

    def take(count):
        taken, scratch[:] = scratch[:count], scratch[count:]
        return taken

    gathered, sent_back = len(gather_cuts), len(return_cuts)
    tokens, outgoing, received = take(gathered), take(gathered), take(gathered)
    results, returned = take(sent_back), take(sent_back)
    sums, arrived = take(sent_back), take(sent_back)
    (
        pick, share, w_in, w_out, gate_w, up_w, down_w, gate_sum, up_sum,
        s_gate, s_up, s_down, s_gate_sum, s_up_sum, s_hidden, mix_rows, acc, tail, prior,
        ws, xs, xr, ins, inr, outs, outr, as_, ar, bs, br, cs, cr, hs, hr, ss, sr, rs, rr,
    ) = scratch
    place = Place(ep_count, tp_count)
    chips, chip, core = place.chips, place.chip, place.core
    devices = ep_count * tp_count
    flat = place.ep * tp_count + place.tp
    after, before = (flat + 1) % devices, (flat + devices - 1) % devices
    after = (after // tp_count, after % tp_count)
    before = (before // tp_count, before % tp_count)
    barrier = pltpu.get_barrier_semaphore()

    def greet(device):
        pl.semaphore_signal(barrier, inc=1, device_id=device, device_id_type=MESH)

    near = [place.sibling(), after, before] + place.peers()
    for device in near:
        greet(device)
    for way in range(2):
        pl.when(place.ahead(way))(lambda way=way: greet(place.side(way)))
    stores = (
        (shared_gate, s_gate.at[0]), (shared_up, s_up.at[0]), (shared_down, s_down.at[0]),
        (mix_w_in, w_in.at[chip, core]), (mix_w_out, w_out.at[chip, core]), (mix_in, mix_rows),
        (exp_gate.at[0], gate_w), (exp_up.at[0], up_w), (exp_down.at[0], down_w),
    )
    loads = [pltpu.make_async_copy(src, dst, ws.at[n]) for n, (src, dst) in enumerate(stores)]
    for load in loads:
        load.start()
    rows, width = moe_in.shape
    capacity = outgoing[0].shape[1]
    slots = ep_count * capacity
    block_rows = tp_count * rows
    g_spans, r_spans = spans_of(width, gather_cuts), spans_of(width, return_cuts)
    sent = []

    normed = rms_rows(moe_in[...], moe_gain[...])
    for c, span in enumerate(g_spans):
        tokens[c][pl.ds(chip, 1), pl.ds(core, 1)] = normed[:, span][None, None]
    pl.semaphore_wait(barrier, len(near) + 2 - jnp.where((chip == 0) | (chip == chips - 1), 1, 0))
    gathers = [LineGather(place, tokens[c], xs.at[c], xr.at[c]) for c in range(gathered)]
    gathers[0].start()
    gathers[1].start()

    shared = []
    for n, buf in enumerate((s_gate, s_up, s_down)):
        loads[n].wait()
        copy = remote(buf.at[0], buf.at[1], cs.at[n], cr.at[n], place.sibling())
        copy.start()
        shared.append(copy)

    top_count = routes.shape[0]
    lines = CORES * ep_count
    line = lax.broadcasted_iota(jnp.int32, (lines, block_rows), 0)
    column = chip * CORES + jnp.where(line < ep_count, core, 1 - core)
    names = (line % ep_count) * tp_count + column
    score_rows = scores[...].astype(jnp.float32)
    score_sum = jnp.sum(score_rows, axis=0, keepdims=True)
    named = jnp.zeros((lines, block_rows), jnp.float32)
    weight = jnp.zeros((lines, block_rows), jnp.float32)
    for k in range(top_count):
        hit = routes[k : k + 1, :] == names
        named = named + jnp.where(hit, 1.0, 0.0)
        weight = weight + jnp.where(hit, score_rows[k : k + 1, :] / score_sum * ROUTED_SCALE, 0.0)
    ones = named.astype(jnp.bfloat16)
    earlier = []
    for low in range(0, block_rows, 512):
        source = lax.broadcasted_iota(jnp.int32, (block_rows, 512), 0)
        target = lax.broadcasted_iota(jnp.int32, (block_rows, 512), 1) + low
        strict = jnp.where(source < target, 1.0, 0.0).astype(jnp.bfloat16)
        earlier.append(jnp.dot(ones, strict, preferred_element_type=jnp.float32))
    spot = jnp.where(named > 0.5, jnp.concatenate(earlier, axis=1), -1.0).astype(jnp.int32)
    slot = lax.broadcasted_iota(jnp.int32, (capacity, block_rows), 0)
    for j in range(ep_count):
        here = spot[j : j + 1, :] == slot
        pick[j * capacity : (j + 1) * capacity, :] = jnp.where(here, 1.0, 0.0).astype(jnp.bfloat16)
    slot = lax.broadcasted_iota(jnp.int32, (capacity, rows), 0)
    for b in range(chips):
        low = b * CORES * rows
        even, odd = slice(low, low + rows), slice(low + rows, low + 2 * rows)
        spots = jnp.where(core == 0, spot[:, even], spot[:, odd])
        weights = jnp.where(core == 0, weight[:, even], weight[:, odd])
        for j in range(lines):
            weighed = jnp.where(spots[j : j + 1, :] == slot, weights[j : j + 1, :], 0.0)
            share[b, :, j * capacity : (j + 1) * capacity] = weighed.T.astype(jnp.bfloat16)

    def scatter(source, landing, c, send, recv):
        for i, (peer, column) in enumerate(place.peers()):
            copy = remote(
                source.at[peer], landing.at[place.ep], send.at[c, i], recv.at[c, i],
                (peer, column),
            )
            copy.start()
            sent.append(copy)
        landing[pl.ds(place.ep, 1)] = source[pl.ds(place.ep, 1)]

    def landing_wait(landing, c, i, send, recv):
        peer = (place.ep - i + ep_count) % ep_count
        block = landing.at[peer]
        remote(block, block, send.at[c, i - 1], recv.at[c, i - 1], (peer, place.tp)).wait_recv()

    first = LineGather(place, w_in, ins, inr)
    second = LineGather(place, w_out, outs, outr)
    edge = (chip == 0) | (chip == chips - 1)
    across = (((1,), (1,)), ((), ()))
    for c, span in enumerate(g_spans):
        cut = span.stop - span.start
        for d in range(1, chips):
            gathers[c].step(d)
            if d == 1 and c + 2 < gathered:
                gathers[c + 2].start()
        if c == 0:
            for load in loads[3:5]:
                load.wait()
            for copy in shared:
                copy.wait_recv()
        if c == min(1, gathered - 1):

            @pl.when(edge)
            def _():
                first.start(False)
                second.start(False)

        gathers[c].arrive()
        picked = jnp.dot(
            pick[...], tokens[c][...].reshape(block_rows, cut), preferred_element_type=jnp.float32
        )
        outgoing[c][...] = picked.astype(jnp.bfloat16).reshape(ep_count, capacity, cut)
        scatter(outgoing[c], received[c], c, as_, ar)
        block = tokens[c][:, pl.ds(core, 1)].reshape(chips * rows, cut)
        for acc_ref, part in ((s_gate_sum, s_gate), (s_up_sum, s_up)):
            value = lax.dot_general(
                block, part[:, :, span].reshape(-1, cut), across,
                preferred_element_type=jnp.float32,
            )
            acc_ref[...] = value if c == 0 else acc_ref[...] + value

    @pl.when(jnp.logical_not(edge))
    def _():
        first.start(False)
        second.start(False)

    first.own_over().start()
    second.own_over().start()
    first.step(1, last=False)
    second.step(1, last=False)

    for load in loads[5:]:
        load.wait()
    for c, span in enumerate(g_spans):
        for i in range(1, ep_count):
            landing_wait(received[c], c, i, as_, ar)
        block = received[c][...].reshape(slots, span.stop - span.start)
        for acc_ref, weights in ((gate_sum, gate_w), (up_sum, up_w)):
            value = jnp.dot(block, weights[span, :], preferred_element_type=jnp.float32)
            acc_ref[...] = value if c == 0 else acc_ref[...] + value
    hidden = (jax.nn.silu(gate_sum[...]) * up_sum[...]).astype(jnp.bfloat16)

    def over(c, i):
        peer = (place.ep - i + ep_count) % ep_count
        return remote(
            returned[c].at[0, peer], returned[c].at[1, peer], ss.at[c, i], sr.at[c, i],
            place.sibling(),
        )

    for c, span in enumerate(r_spans):
        value = jnp.dot(hidden, down_w[:, span], preferred_element_type=jnp.float32)
        results[c][...] = value.astype(jnp.bfloat16).reshape(ep_count, capacity, -1)
        scatter(results[c], returned[c].at[0], c, bs, br)
        over(c, 0).start()
    s_hidden[...] = (
        (jax.nn.silu(s_gate_sum[...]) * s_up_sum[...])
        .astype(jnp.bfloat16)
        .reshape(chips, rows, -1)
    )
    for d in range(2, chips):
        first.step(d, last=False)

    def routed(c, b):
        span = r_spans[c]
        cut = span.stop - span.start
        value = jnp.dot(
            share[b], returned[c][...].reshape(CORES * slots, cut),
            preferred_element_type=jnp.float32,
        )
        extra = jnp.dot(
            s_hidden[b], s_down[:, :, span].reshape(-1, cut), preferred_element_type=jnp.float32
        )
        acc[:, :cut] = value + extra

    def landed(c, way, d):
        n = place.key(way, d)
        block = arrived[c].at[n]
        remote(block, block, rs.at[c, n], rr.at[c, n], place.sibling()).wait_recv()
        cut = block.shape[1]
        acc[:, :cut] = acc[:, :cut] + arrived[c][n].astype(jnp.float32)

    def outward(c, way, d):
        n = place.key(way, d)
        return remote(
            sums[c].at[n], arrived[c].at[n], rs.at[c, n], rr.at[c, n], place.side(way)
        )

    def send_sum(c, way, d, joined):
        routed(c, place.target(way, d))
        if joined:
            landed(c, way, d + 1)
        cut = r_spans[c].stop - r_spans[c].start
        sums[c][place.key(way, d)] = acc[:, :cut].astype(jnp.bfloat16)
        outward(c, way, d).start()

    def from_edge(c, d):
        for way in range(2):
            pl.when(place.beyond(way, d) & jnp.logical_not(place.ahead(1 - way)))(
                lambda way=way: send_sum(c, way, d, False)
            )

    def from_middle(c, d):
        for way in range(2):
            pl.when(place.beyond(way, d) & place.ahead(1 - way))(
                lambda way=way: send_sum(c, way, d, True)
            )

    def far_middle(c):
        for d in range(chips - 2, 1, -1):
            from_middle(c, d)

    for c in range(sent_back):
        for i in range(1, ep_count):
            landing_wait(returned[c].at[0], c, i, bs, br)
            over(c, i).start()
        for i in range(ep_count):
            peer = (place.ep - i + ep_count) % ep_count
            block = returned[c].at[1, peer]
            remote(block, block, ss.at[c, i], sr.at[c, i], place.sibling()).wait_recv()
        for d in range(chips - 1, 1, -1):
            from_edge(c, d)
        if c == 0:
            for d in range(2, chips):
                second.step(d, last=False)
        else:
            far_middle(c - 1)
    far_middle(sent_back - 1)
    for c in range(sent_back):
        from_edge(c, 1)
        from_middle(c, 1)

    for d in range(1, chips):
        first.step(d, onward=False)
    first.arrive()
    groups, group_ch = pool_mat.shape[0], pool_mat.shape[1]
    reach = 2**groups
    mix_normed = rms_rows(mix_rows[...], mix_gain[...])
    projected = jnp.dot(
        mix_normed, w_in[...].reshape(width, groups * group_ch), preferred_element_type=jnp.float32
    ).astype(jnp.bfloat16)
    tail[...] = projected[rows - reach :]
    halo = remote(tail, prior, hs, hr, after)
    halo.start()
    for d in range(1, chips):
        second.step(d, onward=False)
    halo.wait()
    first_row = flat * rows
    keep = jnp.where(first_row % seq_len == 0, 0.0, 1.0)
    extended = jnp.concatenate(
        [prior[...].astype(jnp.float32) * keep, projected.astype(jnp.float32)], axis=0
    )
    position = (first_row + lax.broadcasted_iota(jnp.int32, (rows, group_ch), 0)) % seq_len
    pooled_parts = []
    for group in range(groups):
        channels = slice(group * group_ch, (group + 1) * group_ch)
        running = extended[:, channels]
        for level in range(group + 1):
            running = running + pltpu.roll(running, 2**level, 0)
        counts = jnp.minimum(position + 1, 2 ** (group + 1)).astype(jnp.float32)
        pooled = (running[reach:] / counts - extended[reach:, channels]).astype(jnp.bfloat16)
        grouped = jnp.dot(pooled, pool_mat[group], preferred_element_type=jnp.float32)
        pooled_parts.append((grouped * pool_scale[:, channels]).astype(jnp.bfloat16))
    pool_out = jnp.concatenate(pooled_parts, axis=1)
    second.arrive()
    span = w_out.shape[3]
    for column in range(tp_count):
        mixed[:, column * span : (column + 1) * span] = jnp.dot(
            pool_out, w_out[column // CORES, column % CORES], preferred_element_type=jnp.float32
        ).astype(jnp.bfloat16)

    for c, span in enumerate(r_spans):
        routed(c, chip)
        for way in range(2):
            pl.when(place.behind(way, 1))(lambda way=way: landed(c, way, 1))
        moe_out[:, span] = acc[:, : span.stop - span.start].astype(jnp.bfloat16)

    for copy in sent + shared:
        copy.wait_send()
    for c in range(sent_back):
        for i in range(ep_count):
            over(c, i).wait_send()
        for way, d in place.keys:
            pl.when(place.beyond(way, d))(
                lambda way=way, d=d: outward(c, way, d).wait_send()
            )
    for gather in gathers + [first, second]:
        gather.close()


def shards(
    mix_in, mix_gain, mix_w_in, pool_mat, pool_scale, mix_w_out, moe_in, moe_gain, routes,
    route_score, exp_gate, exp_up, exp_down, shared_gate, shared_up, shared_down,
):
    ep_count, tp_count = lax.axis_size("ep"), lax.axis_size("tp")
    rows, width = moe_in.shape
    block_rows, top_count = routes.shape
    capacity = 2 * block_rows * top_count // (ep_count * tp_count)
    slots = ep_count * capacity
    dma = lambda *shape: pltpu.SemaphoreType.DMA(shape)
    bf16, f32 = jnp.bfloat16, jnp.float32

    chips = tp_count // CORES
    messages = 2 * (chips - 1)
    hidden, s_hidden = exp_gate.shape[2], shared_gate.shape[0]
    reach = 2 ** pool_mat.shape[0]
    seq_len = mix_in.shape[0] * ep_count * tp_count // SEQS_MIX
    buffer = lambda *shape: pltpu.VMEM(shape, bf16)
    g_cuts = [s.stop - s.start for s in spans_of(width, GATHER_CUTS)]
    r_cuts = [s.stop - s.start for s in spans_of(width, RETURN_CUTS)]
    gathered, sent_back = len(g_cuts), len(r_cuts)
    mixed, moe_out = pl.pallas_call(
        functools.partial(layer_kernel, ep_count, tp_count, seq_len, GATHER_CUTS, RETURN_CUTS),
        out_shape=[
            jax.ShapeDtypeStruct(mix_in.shape, bf16),
            jax.ShapeDtypeStruct(moe_in.shape, bf16),
        ],
        in_specs=[pl.BlockSpec(memory_space=pltpu.VMEM)] * 7
        + [pl.BlockSpec(memory_space=pl.ANY)] * 9,
        out_specs=[pl.BlockSpec(memory_space=pltpu.VMEM)] * 2,
        scratch_shapes=[buffer(chips, CORES, rows, cut) for cut in g_cuts]
        + [buffer(ep_count, capacity, cut) for cut in g_cuts] * 2
        + [buffer(ep_count, capacity, cut) for cut in r_cuts]
        + [buffer(CORES, ep_count, capacity, cut) for cut in r_cuts]
        + [buffer(messages, rows, cut) for cut in r_cuts] * 2
        + [
            buffer(slots, block_rows),
            buffer(chips, rows, CORES * slots),
            buffer(chips, CORES, *mix_w_in.shape),
            buffer(chips, CORES, *mix_w_out.shape),
            buffer(width, hidden),
            buffer(width, hidden),
            buffer(hidden, width),
            pltpu.VMEM((slots, hidden), f32),
            pltpu.VMEM((slots, hidden), f32),
            buffer(CORES, *shared_gate.shape),
            buffer(CORES, *shared_up.shape),
            buffer(CORES, *shared_down.shape),
            pltpu.VMEM((chips * rows, CORES * s_hidden), f32),
            pltpu.VMEM((chips * rows, CORES * s_hidden), f32),
            buffer(chips, rows, CORES * s_hidden),
            buffer(*mix_in.shape),
            pltpu.VMEM((rows, max(r_cuts)), f32),
            buffer(reach, mix_w_in.shape[1]),
            buffer(reach, mix_w_in.shape[1]),
            dma(9),
            dma(gathered, 2 * messages + 1),
            dma(gathered, 2 * messages + 1),
        ]
        + [dma(2 * messages + 1)] * 4
        + [dma(gathered, ep_count - 1)] * 2
        + [dma(sent_back, ep_count - 1)] * 2
        + [dma(3), dma(3)]
        + [pltpu.SemaphoreType.DMA, pltpu.SemaphoreType.DMA]
        + [dma(sent_back, ep_count)] * 2
        + [dma(sent_back, messages)] * 2,
        compiler_params=pltpu.CompilerParams(
            collective_id=0, has_side_effects=True, vmem_limit_bytes=67043328
        ),
    )(
        moe_in, moe_gain[None, :], routes.T, route_score.T, mix_gain[None, :], pool_mat,
        pool_scale[None, :], shared_gate, shared_up, shared_down, mix_w_in, mix_w_out, mix_in,
        exp_gate, exp_up, exp_down,
    )
    return (mixed, moe_out)


def solution(mesh):
    return jax.shard_map(
        shards,
        mesh=mesh,
        in_specs=(
            P(("ep", "tp"), None),
            P(),
            P("tp", None),
            P(),
            P(),
            P(None, "tp"),
            P(("ep", "tp"), None),
            P(),
            P("ep", None),
            P("ep", None),
            P(("ep", "tp"), None, None),
            P(("ep", "tp"), None, None),
            P(("ep", "tp"), None, None),
            P("tp", None),
            P("tp", None),
            P("tp", None),
        ),
        out_specs=(P(("ep", "tp"), None), P(("ep", "tp"), None)),
        check_vma=False,
    )
```

time: 132 us -> 110 us (0.83)
  Pallas kernels: 126 us -> 106 us
    pallas_call x1, Pallas kernels: 126 us -> 106 us  [shards(): pl.pallas_call(functools.partial(layer_kernel, ep_count, tp_count, seq_le...]
where the time goes in v1:
time: 110 us
  Pallas kernels  106 us (96%)
  local copies, waits for them, and re-layouts  3.76 us (3%)
    pallas_call x1, Pallas kernels, shards(): pl.pallas_call(functools.partial(layer_kernel, ep_count, tp_count, seq_le...  106 us
    unnamed x2, local copies, waits for them, and re-layouts  3.76 us

profile of v1, /device:TPU:0, one launch (start us, length us, event | category | flops | bytes accessed | tf_op | source)
XLA Modules:
  0.0 110.3 jit_solution(6898075490539810683)
XLA Ops:
  0.6 105.8 %shard_map.167 = (bf16[128,2048]{1,0:T(8,128)(2,1)}, bf16[128,2048]{1,0:T(8,128)(2,1)}) custom-call(bf16[128,2048]{1,0:T(8,128)(2,1)} %moe_in.1, f32[1,2048]{1,0:T(1,128)} %bitcast.5, s32[2,1024]{1,0:T(2,128)} %bitcast.6, bf16[2,1024]{1,0:T(2,128)(2,1)} %bitcast.8, f32[1,2048]{1,0:T(1,128)} %bitcast.7, bf16[4,128,128]{2,1,0:T(8,128)(2,1)} %pool_mat.1, ...), custom_call_target="tpu_custom_call" | custom-call | tf_op jit(solution)/shard_map/pallas_call | solution.py:509
  106.5 1.9 %copy.20 = bf16[128,2048]{1,0:T(8,128)(2,1)} copy(bf16[128,2048]{1,0:T(8,128)(2,1)} %get-tuple-element.4) | data formatting | bytes 1048576
  108.4 1.9 %copy.21 = bf16[128,2048]{1,0:T(8,128)(2,1)} copy(bf16[128,2048]{1,0:T(8,128)(2,1)} %get-tuple-element.5) | data formatting | bytes 1048576

commit v2 on v1

--- a/solution.py
+++ b/solution.py
@@ -13,8 +13,9 @@
 NORM_EPS = 1e-06
 ROUTED_SCALE = 2.5
 MESH = pl.DeviceIdType.MESH
-GATHER_CUTS = (4, 4, 4, 4)
-RETURN_CUTS = (4, 4, 4, 4)
+AHEAD = 2
+GATHER_CUTS = (1, 1, 1, 1, 1, 1, 1, 1)
+RETURN_CUTS = (1, 1, 2, 2, 1, 1)
 
 
 def rms_rows(values, gain):
@@ -69,6 +70,9 @@
     def target(self, way, d):
         return self.chip + d if way == 0 else self.chip - d
 
+    def edge(self, chip):
+        return (chip == 0) | (chip == self.chips - 1)
+
     def side(self, way):
         return (self.ep, self.target(way, 1) * CORES + self.core)
 
@@ -108,9 +112,11 @@
         if over:
             self.own_over().start()
 
-    def step(self, d, onward=True, last=True):
+    def step(self, d, onward=True, last=True, edge=None):
         place = self.place
         for way in range(2):
+            outer = place.edge(place.origin(way, d))
+            chosen = True if edge is None else outer == edge
 
             def receive(way=way):
                 n = place.key(way, d)
@@ -130,7 +136,7 @@
                 self.pass_over(way, d).start()
 
             if onward:
-                pl.when(place.behind(way, d) & place.ahead(way))(forward)
+                pl.when(place.behind(way, d) & place.ahead(way) & chosen)(forward)
             if last:
                 pl.when(place.behind(way, d) & jnp.logical_not(place.ahead(way)))(finish)
 
@@ -164,7 +170,7 @@
 
 def layer_kernel(
     ep_count, tp_count, seq_len, gather_cuts, return_cuts,
-    moe_in, moe_gain, routes, scores, mix_gain, pool_mat, pool_scale,
+    moe_gain_in, routes_in, scores_in, mix_gain_in, pool_scale_in, moe_in, pool_mat,
     shared_gate, shared_up, shared_down, mix_w_in, mix_w_out, mix_in, exp_gate, exp_up, exp_down,
     mixed, moe_out,
     *scratch,
@@ -181,7 +187,8 @@
     sums, arrived = take(sent_back), take(sent_back)
     (
         pick, share, w_in, w_out, gate_w, up_w, down_w, gate_sum, up_sum,
-        s_gate, s_up, s_down, s_gate_sum, s_up_sum, s_hidden, mix_rows, acc, tail, prior,
+        s_gate, s_up, s_down, s_gate_sum, s_up_sum, s_hidden, moe_rows, mix_rows, mats, acc, own,
+        moe_gain, routes, scores, mix_gain, pool_scale,
         ws, xs, xr, ins, inr, outs, outr, as_, ar, bs, br, cs, cr, hs, hr, ss, sr, rs, rr,
     ) = scratch
     place = Place(ep_count, tp_count)
@@ -196,41 +203,51 @@
     def greet(device):
         pl.semaphore_signal(barrier, inc=1, device_id=device, device_id_type=MESH)
 
+    rows, width = moe_in.shape
+    reach = mix_rows.shape[0] - rows
+    stores = (
+        (moe_in, moe_rows), (moe_gain_in, moe_gain), (routes_in, routes), (scores_in, scores),
+        (shared_gate, s_gate.at[0]), (shared_up, s_up.at[0]), (shared_down, s_down.at[0]),
+        (mix_w_in, w_in.at[chip, core]), (mix_w_out, w_out.at[chip, core]),
+        (mix_in, mix_rows.at[pl.ds(reach, rows)]), (pool_mat, mats),
+        (mix_gain_in, mix_gain), (pool_scale_in, pool_scale),
+        (exp_gate.at[0], gate_w), (exp_up.at[0], up_w), (exp_down.at[0], down_w),
+    )
+    loads = [pltpu.make_async_copy(src, dst, ws.at[n]) for n, (src, dst) in enumerate(stores)]
+    for load in loads[:4]:
+        load.start()
     near = [place.sibling(), after, before] + place.peers()
     for device in near:
         greet(device)
     for way in range(2):
         pl.when(place.ahead(way))(lambda way=way: greet(place.side(way)))
-    stores = (
-        (shared_gate, s_gate.at[0]), (shared_up, s_up.at[0]), (shared_down, s_down.at[0]),
-        (mix_w_in, w_in.at[chip, core]), (mix_w_out, w_out.at[chip, core]), (mix_in, mix_rows),
-        (exp_gate.at[0], gate_w), (exp_up.at[0], up_w), (exp_down.at[0], down_w),
-    )
-    loads = [pltpu.make_async_copy(src, dst, ws.at[n]) for n, (src, dst) in enumerate(stores)]
-    for load in loads:
+    for load in loads[4:]:
         load.start()
-    rows, width = moe_in.shape
     capacity = outgoing[0].shape[1]
     slots = ep_count * capacity
     block_rows = tp_count * rows
     g_spans, r_spans = spans_of(width, gather_cuts), spans_of(width, return_cuts)
     sent = []
 
-    normed = rms_rows(moe_in[...], moe_gain[...])
+    loads[0].wait()
+    loads[1].wait()
+    normed = rms_rows(moe_rows[...], moe_gain[...])
     for c, span in enumerate(g_spans):
         tokens[c][pl.ds(chip, 1), pl.ds(core, 1)] = normed[:, span][None, None]
     pl.semaphore_wait(barrier, len(near) + 2 - jnp.where((chip == 0) | (chip == chips - 1), 1, 0))
     gathers = [LineGather(place, tokens[c], xs.at[c], xr.at[c]) for c in range(gathered)]
-    gathers[0].start()
-    gathers[1].start()
+    for c in range(AHEAD):
+        gathers[c].start()
 
     shared = []
     for n, buf in enumerate((s_gate, s_up, s_down)):
-        loads[n].wait()
+        loads[4 + n].wait()
         copy = remote(buf.at[0], buf.at[1], cs.at[n], cr.at[n], place.sibling())
         copy.start()
         shared.append(copy)
 
+    loads[2].wait()
+    loads[3].wait()
     top_count = routes.shape[0]
     lines = CORES * ep_count
     line = lax.broadcasted_iota(jnp.int32, (lines, block_rows), 0)
@@ -283,59 +300,79 @@
 
     first = LineGather(place, w_in, ins, inr)
     second = LineGather(place, w_out, outs, outr)
-    edge = (chip == 0) | (chip == chips - 1)
+    edge = place.edge(chip)
     across = (((1,), (1,)), ((), ()))
-    for c, span in enumerate(g_spans):
-        cut = span.stop - span.start
-        for d in range(1, chips):
-            gathers[c].step(d)
-            if d == 1 and c + 2 < gathered:
-                gathers[c + 2].start()
-        if c == 0:
-            for load in loads[3:5]:
-                load.wait()
-            for copy in shared:
-                copy.wait_recv()
-        if c == min(1, gathered - 1):
-
-            @pl.when(edge)
-            def _():
-                first.start(False)
-                second.start(False)
-
-        gathers[c].arrive()
-        picked = jnp.dot(
-            pick[...], tokens[c][...].reshape(block_rows, cut), preferred_element_type=jnp.float32
-        )
-        outgoing[c][...] = picked.astype(jnp.bfloat16).reshape(ep_count, capacity, cut)
-        scatter(outgoing[c], received[c], c, as_, ar)
-        block = tokens[c][:, pl.ds(core, 1)].reshape(chips * rows, cut)
-        for acc_ref, part in ((s_gate_sum, s_gate), (s_up_sum, s_up)):
-            value = lax.dot_general(
-                block, part[:, :, span].reshape(-1, cut), across,
-                preferred_element_type=jnp.float32,
-            )
-            acc_ref[...] = value if c == 0 else acc_ref[...] + value
-
-    @pl.when(jnp.logical_not(edge))
-    def _():
-        first.start(False)
-        second.start(False)
-
-    first.own_over().start()
-    second.own_over().start()
-    first.step(1, last=False)
-    second.step(1, last=False)
-
-    for load in loads[5:]:
-        load.wait()
-    for c, span in enumerate(g_spans):
+
+    def gate_up(c):
+        span = g_spans[c]
         for i in range(1, ep_count):
             landing_wait(received[c], c, i, as_, ar)
         block = received[c][...].reshape(slots, span.stop - span.start)
         for acc_ref, weights in ((gate_sum, gate_w), (up_sum, up_w)):
             value = jnp.dot(block, weights[span, :], preferred_element_type=jnp.float32)
             acc_ref[...] = value if c == 0 else acc_ref[...] + value
+
+    lag = 3
+    for turn in range(gathered + chips - 2):
+        for d in range(1, chips):
+            if 0 <= turn - (d - 1) < gathered:
+                gathers[turn - (d - 1)].step(d)
+            if d == 1 and turn + AHEAD < gathered:
+                gathers[turn + AHEAD].start()
+        if turn == 0:
+            for load in loads[7:13]:
+                load.wait()
+            for copy in shared:
+                copy.wait_recv()
+        if turn == max(0, gathered - 1 - AHEAD):
+
+            @pl.when(edge)
+            def _():
+                first.start(False)
+                second.start(False)
+
+        c = turn - (chips - 2)
+        if c < 0:
+            continue
+        gathers[c].arrive()
+        cut = g_spans[c].stop - g_spans[c].start
+        picked = jnp.dot(
+            pick[...], tokens[c][...].reshape(block_rows, cut), preferred_element_type=jnp.float32
+        )
+        outgoing[c][...] = picked.astype(jnp.bfloat16).reshape(ep_count, capacity, cut)
+        scatter(outgoing[c], received[c], c, as_, ar)
+        if c == lag:
+            for load in loads[13:]:
+                load.wait()
+        if c >= lag:
+            gate_up(c - lag)
+
+    @pl.when(jnp.logical_not(edge))
+    def _():
+        first.start(False)
+        second.start(False)
+
+    first.step(1, last=False, edge=True)
+    second.step(1, last=False, edge=True)
+    first.own_over().start()
+    second.own_over().start()
+    halo = remote(
+        mix_rows.at[pl.ds(rows, reach)], mix_rows.at[pl.ds(0, reach)], hs, hr, after
+    )
+    halo.start()
+
+    for c in range(gathered - lag, gathered - 1):
+        gate_up(c)
+    for acc_ref, part in ((s_gate_sum, s_gate), (s_up_sum, s_up)):
+        value = 0.0
+        for c, span in enumerate(g_spans):
+            value = value + lax.dot_general(
+                tokens[c][:, pl.ds(core, 1)].reshape(chips * rows, -1),
+                part[:, :, span].reshape(-1, span.stop - span.start), across,
+                preferred_element_type=jnp.float32,
+            )
+        acc_ref[...] = value
+    gate_up(gathered - 1)
     hidden = (jax.nn.silu(gate_sum[...]) * up_sum[...]).astype(jnp.bfloat16)
 
     def over(c, i):
@@ -355,8 +392,7 @@
         .astype(jnp.bfloat16)
         .reshape(chips, rows, -1)
     )
-    for d in range(2, chips):
-        first.step(d, last=False)
+    first.step(1, last=False, edge=False)
 
     def routed(c, b):
         span = r_spans[c]
@@ -370,43 +406,57 @@
         )
         acc[:, :cut] = value + extra
 
-    def landed(c, way, d):
+    def leaving(way, d):
+        return d - 1 if way == 0 else chips - 1 - d
+
+    def reaching(way, d):
+        return d - 1 if way == 0 else chips + 1 - d
+
+    def landed(c, way, d, total):
         n = place.key(way, d)
-        block = arrived[c].at[n]
+        block = arrived[c].at[reaching(way, d)]
         remote(block, block, rs.at[c, n], rr.at[c, n], place.sibling()).wait_recv()
-        cut = block.shape[1]
-        acc[:, :cut] = acc[:, :cut] + arrived[c][n].astype(jnp.float32)
+        total[...] = total[...] + arrived[c][reaching(way, d)].astype(jnp.float32)
 
     def outward(c, way, d):
         n = place.key(way, d)
         return remote(
-            sums[c].at[n], arrived[c].at[n], rs.at[c, n], rr.at[c, n], place.side(way)
+            sums[c].at[leaving(way, d)], arrived[c].at[reaching(way, d)], rs.at[c, n],
+            rr.at[c, n], place.side(way),
         )
 
-    def send_sum(c, way, d, joined):
-        routed(c, place.target(way, d))
-        if joined:
-            landed(c, way, d + 1)
-        cut = r_spans[c].stop - r_spans[c].start
-        sums[c][place.key(way, d)] = acc[:, :cut].astype(jnp.bfloat16)
-        outward(c, way, d).start()
-
     def from_edge(c, d):
-        for way in range(2):
-            pl.when(place.beyond(way, d) & jnp.logical_not(place.ahead(1 - way)))(
-                lambda way=way: send_sum(c, way, d, False)
-            )
+        @pl.when(edge)
+        def _():
+            up = chip == 0
+            pick_way = lambda low, high: jnp.where(up, low, high)
+            routed(c, pick_way(place.target(0, d), place.target(1, d)))
+            slot = pick_way(leaving(0, d), leaving(1, d))
+            cut = r_spans[c].stop - r_spans[c].start
+            sums[c][pl.ds(slot, 1)] = acc[:, :cut].astype(jnp.bfloat16)[None]
+            n = pick_way(place.key(0, d), place.key(1, d))
+            remote(
+                sums[c].at[slot], arrived[c].at[pick_way(reaching(0, d), reaching(1, d))],
+                rs.at[c, n], rr.at[c, n],
+                (place.ep, pick_way(place.target(0, 1), place.target(1, 1)) * CORES + core),
+            ).start()
 
     def from_middle(c, d):
         for way in range(2):
-            pl.when(place.beyond(way, d) & place.ahead(1 - way))(
-                lambda way=way: send_sum(c, way, d, True)
-            )
+
+            @pl.when(place.beyond(way, d) & place.ahead(1 - way))
+            def _(way=way):
+                routed(c, place.target(way, d))
+                cut = r_spans[c].stop - r_spans[c].start
+                landed(c, way, d + 1, acc.at[:, :cut])
+                sums[c][leaving(way, d)] = acc[:, :cut].astype(jnp.bfloat16)
+                outward(c, way, d).start()
 
     def far_middle(c):
         for d in range(chips - 2, 1, -1):
             from_middle(c, d)
 
+    last = sent_back - 1
     for c in range(sent_back):
         for i in range(1, ep_count):
             landing_wait(returned[c].at[0], c, i, bs, br)
@@ -415,38 +465,40 @@
             peer = (place.ep - i + ep_count) % ep_count
             block = returned[c].at[1, peer]
             remote(block, block, ss.at[c, i], sr.at[c, i], place.sibling()).wait_recv()
-        for d in range(chips - 1, 1, -1):
+        for d in range(chips - 1, 0 if c < last - 3 else 1, -1):
             from_edge(c, d)
         if c == 0:
-            for d in range(2, chips):
-                second.step(d, last=False)
-        else:
+            second.step(1, last=False, edge=False)
+        for gather, turn in ((first, 1), (second, 2)):
+            if c == min(last, turn):
+                for d in range(2, chips):
+                    gather.step(d, last=False)
+        if c > 0:
             far_middle(c - 1)
-    far_middle(sent_back - 1)
-    for c in range(sent_back):
+        if c > 1:
+            from_middle(c - 2, 1)
+    far_middle(last)
+    for c in range(max(0, last - 3), sent_back):
         from_edge(c, 1)
+    for c in range(max(0, last - 1), sent_back):
         from_middle(c, 1)
+    for c, span in enumerate(r_spans):
+        routed(c, chip)
+        own[:, span] = acc[:, : span.stop - span.start]
 
     for d in range(1, chips):
         first.step(d, onward=False)
     first.arrive()
-    groups, group_ch = pool_mat.shape[0], pool_mat.shape[1]
-    reach = 2**groups
+    halo.wait_recv()
+    groups, group_ch = mats.shape[0], mats.shape[1]
     mix_normed = rms_rows(mix_rows[...], mix_gain[...])
     projected = jnp.dot(
         mix_normed, w_in[...].reshape(width, groups * group_ch), preferred_element_type=jnp.float32
     ).astype(jnp.bfloat16)
-    tail[...] = projected[rows - reach :]
-    halo = remote(tail, prior, hs, hr, after)
-    halo.start()
-    for d in range(1, chips):
-        second.step(d, onward=False)
-    halo.wait()
     first_row = flat * rows
     keep = jnp.where(first_row % seq_len == 0, 0.0, 1.0)
-    extended = jnp.concatenate(
-        [prior[...].astype(jnp.float32) * keep, projected.astype(jnp.float32)], axis=0
-    )
+    projected = projected.astype(jnp.float32)
+    extended = jnp.concatenate([projected[:reach] * keep, projected[reach:]], axis=0)
     position = (first_row + lax.broadcasted_iota(jnp.int32, (rows, group_ch), 0)) % seq_len
     pooled_parts = []
     for group in range(groups):
@@ -456,9 +508,11 @@
             running = running + pltpu.roll(running, 2**level, 0)
         counts = jnp.minimum(position + 1, 2 ** (group + 1)).astype(jnp.float32)
         pooled = (running[reach:] / counts - extended[reach:, channels]).astype(jnp.bfloat16)
-        grouped = jnp.dot(pooled, pool_mat[group], preferred_element_type=jnp.float32)
+        grouped = jnp.dot(pooled, mats[group], preferred_element_type=jnp.float32)
         pooled_parts.append((grouped * pool_scale[:, channels]).astype(jnp.bfloat16))
     pool_out = jnp.concatenate(pooled_parts, axis=1)
+    for d in range(1, chips):
+        second.step(d, onward=False)
     second.arrive()
     span = w_out.shape[3]
     for column in range(tp_count):
@@ -467,11 +521,15 @@
         ).astype(jnp.bfloat16)
 
     for c, span in enumerate(r_spans):
-        routed(c, chip)
         for way in range(2):
-            pl.when(place.behind(way, 1))(lambda way=way: landed(c, way, 1))
-        moe_out[:, span] = acc[:, : span.stop - span.start].astype(jnp.bfloat16)
-
+
+            def join(way=way):
+                landed(c, way, 1, own.at[:, span])
+
+            pl.when(place.behind(way, 1))(join)
+        moe_out[:, span] = own[:, span].astype(jnp.bfloat16)
+
+    halo.wait_send()
     for copy in sent + shared:
         copy.wait_send()
     for c in range(sent_back):
@@ -506,20 +564,13 @@
     g_cuts = [s.stop - s.start for s in spans_of(width, GATHER_CUTS)]
     r_cuts = [s.stop - s.start for s in spans_of(width, RETURN_CUTS)]
     gathered, sent_back = len(g_cuts), len(r_cuts)
-    mixed, moe_out = pl.pallas_call(
-        functools.partial(layer_kernel, ep_count, tp_count, seq_len, GATHER_CUTS, RETURN_CUTS),
-        out_shape=[
-            jax.ShapeDtypeStruct(mix_in.shape, bf16),
-            jax.ShapeDtypeStruct(moe_in.shape, bf16),
-        ],
-        in_specs=[pl.BlockSpec(memory_space=pltpu.VMEM)] * 7
-        + [pl.BlockSpec(memory_space=pl.ANY)] * 9,
-        out_specs=[pl.BlockSpec(memory_space=pltpu.VMEM)] * 2,
-        scratch_shapes=[buffer(chips, CORES, rows, cut) for cut in g_cuts]
+    scratch = (
+        [buffer(chips, CORES, rows, cut) for cut in g_cuts]
         + [buffer(ep_count, capacity, cut) for cut in g_cuts] * 2
         + [buffer(ep_count, capacity, cut) for cut in r_cuts]
         + [buffer(CORES, ep_count, capacity, cut) for cut in r_cuts]
-        + [buffer(messages, rows, cut) for cut in r_cuts] * 2
+        + [buffer(chips - 1, rows, cut) for cut in r_cuts]
+        + [buffer(chips + 1, rows, cut) for cut in r_cuts]
         + [
             buffer(slots, block_rows),
             buffer(chips, rows, CORES * slots),
@@ -536,11 +587,17 @@
             pltpu.VMEM((chips * rows, CORES * s_hidden), f32),
             pltpu.VMEM((chips * rows, CORES * s_hidden), f32),
             buffer(chips, rows, CORES * s_hidden),
-            buffer(*mix_in.shape),
+            buffer(*moe_in.shape),
+            buffer(mix_in.shape[0] + reach, width),
+            buffer(*pool_mat.shape),
             pltpu.VMEM((rows, max(r_cuts)), f32),
-            buffer(reach, mix_w_in.shape[1]),
-            buffer(reach, mix_w_in.shape[1]),
-            dma(9),
+            pltpu.VMEM((rows, width), f32),
+            pltpu.VMEM((1, width), f32),
+            pltpu.VMEM((top_count, block_rows), routes.dtype),
+            buffer(top_count, block_rows),
+            pltpu.VMEM((1, width), f32),
+            pltpu.VMEM((1, pool_scale.shape[0]), f32),
+            dma(16),
             dma(gathered, 2 * messages + 1),
             dma(gathered, 2 * messages + 1),
         ]
@@ -550,13 +607,23 @@
         + [dma(3), dma(3)]
         + [pltpu.SemaphoreType.DMA, pltpu.SemaphoreType.DMA]
         + [dma(sent_back, ep_count)] * 2
-        + [dma(sent_back, messages)] * 2,
+        + [dma(sent_back, messages)] * 2
+    )
+    mixed, moe_out = pl.pallas_call(
+        functools.partial(layer_kernel, ep_count, tp_count, seq_len, GATHER_CUTS, RETURN_CUTS),
+        out_shape=[
+            jax.ShapeDtypeStruct(mix_in.shape, bf16),
+            jax.ShapeDtypeStruct(moe_in.shape, bf16),
+        ],
+        in_specs=[pl.BlockSpec(memory_space=pltpu.HBM)] * 16,
+        out_specs=[pl.BlockSpec(memory_space=pltpu.VMEM)] * 2,
+        scratch_shapes=scratch,
         compiler_params=pltpu.CompilerParams(
             collective_id=0, has_side_effects=True, vmem_limit_bytes=67043328
         ),
     )(
-        moe_in, moe_gain[None, :], routes.T, route_score.T, mix_gain[None, :], pool_mat,
-        pool_scale[None, :], shared_gate, shared_up, shared_down, mix_w_in, mix_w_out, mix_in,
+        moe_gain[None, :], routes.T, route_score.T, mix_gain[None, :], pool_scale[None, :],
+        moe_in, pool_mat, shared_gate, shared_up, shared_down, mix_w_in, mix_w_out, mix_in,
         exp_gate, exp_up, exp_down,
     )
     return (mixed, moe_out)

time: 110 us -> 104 us (0.945)
  Pallas kernels: 106 us -> 99.7 us
    pallas_call x1, Pallas kernels: 106 us -> 99.7 us  [shards(): pl.pallas_call(functools.partial(layer_kernel, ep_count, tp_count, seq_le...]
where the time goes in v2:
time: 104 us
  Pallas kernels  99.7 us (96%)
  local copies, waits for them, and re-layouts  3.76 us (4%)
    pallas_call x1, Pallas kernels, shards(): pl.pallas_call(functools.partial(layer_kernel, ep_count, tp_count, seq_le...  99.7 us
    unnamed x2, local copies, waits for them, and re-layouts  3.76 us

profile of v2, /device:TPU:0, one launch (start us, length us, event | category | flops | bytes accessed | tf_op | source)
XLA Modules:
  0.0 104.1 jit_solution(15712602042491799493)
XLA Ops:
  0.6 99.7 %shard_map.167 = (bf16[128,2048]{1,0:T(8,128)(2,1)}, bf16[128,2048]{1,0:T(8,128)(2,1)}) custom-call(f32[1,2048]{1,0:T(1,128)} %bitcast.5, s32[2,1024]{1,0:T(2,128)} %bitcast.6, bf16[2,1024]{1,0:T(2,128)(2,1)} %bitcast.8, f32[1,2048]{1,0:T(1,128)} %bitcast.7, f32[1,512]{1,0:T(1,128)} %bitcast.9, bf16[128,2048]{1,0:T(8,128)(2,1)} %moe_in.1, ...), custom_call_target="tpu_custom_call" | custom-call | tf_op jit(solution)/shard_map/pallas_call | solution.py:612
  100.3 1.9 %copy.20 = bf16[128,2048]{1,0:T(8,128)(2,1)} copy(bf16[128,2048]{1,0:T(8,128)(2,1)} %get-tuple-element.4) | data formatting | bytes 1048576
  102.2 1.9 %copy.21 = bf16[128,2048]{1,0:T(8,128)(2,1)} copy(bf16[128,2048]{1,0:T(8,128)(2,1)} %get-tuple-element.5) | data formatting | bytes 1048576

commit v3 on v2

--- a/solution.py
+++ b/solution.py
@@ -14,8 +14,12 @@
 ROUTED_SCALE = 2.5
 MESH = pl.DeviceIdType.MESH
 AHEAD = 2
+LEAD = 5
+PROMPT = 2
+VMEM_BYTES = 67043328
+CHUNKS = 4
 GATHER_CUTS = (1, 1, 1, 1, 1, 1, 1, 1)
-RETURN_CUTS = (1, 1, 2, 2, 1, 1)
+RETURN_CUTS = (1, 1, 2, 2, 2, 2, 2, 2, 2)
 
 
 def rms_rows(values, gain):
@@ -79,8 +83,15 @@
     def sibling(self):
         return (self.ep, self.chip * CORES + 1 - self.core)
 
-    def peers(self):
-        return [((self.ep + i) % self.ep_count, self.tp) for i in range(1, self.ep_count)]
+    def partner(self, i):
+        peer, bit = 0, 1
+        while bit < self.ep_count:
+            peer = peer + (self.ep // bit + i // bit) % 2 * bit
+            bit *= 2
+        return peer
+
+    def turns(self):
+        return range(self.ep_count - 1, 0, -1)
 
 
 class LineGather:
@@ -172,7 +183,7 @@
     ep_count, tp_count, seq_len, gather_cuts, return_cuts,
     moe_gain_in, routes_in, scores_in, mix_gain_in, pool_scale_in, moe_in, pool_mat,
     shared_gate, shared_up, shared_down, mix_w_in, mix_w_out, mix_in, exp_gate, exp_up, exp_down,
-    mixed, moe_out,
+    mixed_out, moe_final,
     *scratch,
 ):
     scratch = list(scratch)
@@ -188,16 +199,15 @@
     (
         pick, share, w_in, w_out, gate_w, up_w, down_w, gate_sum, up_sum,
         s_gate, s_up, s_down, s_gate_sum, s_up_sum, s_hidden, moe_rows, mix_rows, mats, acc, own,
-        moe_gain, routes, scores, mix_gain, pool_scale,
+        moe_gain, routes, scores, mix_gain, pool_scale, mixed, moe_out, os,
         ws, xs, xr, ins, inr, outs, outr, as_, ar, bs, br, cs, cr, hs, hr, ss, sr, rs, rr,
     ) = scratch
     place = Place(ep_count, tp_count)
     chips, chip, core = place.chips, place.chip, place.core
     devices = ep_count * tp_count
     flat = place.ep * tp_count + place.tp
-    after, before = (flat + 1) % devices, (flat + devices - 1) % devices
+    after = (flat + 1) % devices
     after = (after // tp_count, after % tp_count)
-    before = (before // tp_count, before % tp_count)
     barrier = pltpu.get_barrier_semaphore()
 
     def greet(device):
@@ -216,7 +226,7 @@
     loads = [pltpu.make_async_copy(src, dst, ws.at[n]) for n, (src, dst) in enumerate(stores)]
     for load in loads[:4]:
         load.start()
-    near = [place.sibling(), after, before] + place.peers()
+    near = [place.sibling()] + [(place.partner(i), place.tp) for i in place.turns()]
     for device in near:
         greet(device)
     for way in range(2):
@@ -284,17 +294,18 @@
             share[b, :, j * capacity : (j + 1) * capacity] = weighed.T.astype(jnp.bfloat16)
 
     def scatter(source, landing, c, send, recv):
-        for i, (peer, column) in enumerate(place.peers()):
+        for i in place.turns():
+            peer = place.partner(i)
             copy = remote(
-                source.at[peer], landing.at[place.ep], send.at[c, i], recv.at[c, i],
-                (peer, column),
+                source.at[peer], landing.at[place.ep], send.at[c, i - 1], recv.at[c, i - 1],
+                (peer, place.tp),
             )
             copy.start()
             sent.append(copy)
         landing[pl.ds(place.ep, 1)] = source[pl.ds(place.ep, 1)]
 
     def landing_wait(landing, c, i, send, recv):
-        peer = (place.ep - i + ep_count) % ep_count
+        peer = place.partner(i)
         block = landing.at[peer]
         remote(block, block, send.at[c, i - 1], recv.at[c, i - 1], (peer, place.tp)).wait_recv()
 
@@ -305,7 +316,7 @@
 
     def gate_up(c):
         span = g_spans[c]
-        for i in range(1, ep_count):
+        for i in place.turns():
             landing_wait(received[c], c, i, as_, ar)
         block = received[c][...].reshape(slots, span.stop - span.start)
         for acc_ref, weights in ((gate_sum, gate_w), (up_sum, up_w)):
@@ -376,17 +387,20 @@
     hidden = (jax.nn.silu(gate_sum[...]) * up_sum[...]).astype(jnp.bfloat16)
 
     def over(c, i):
-        peer = (place.ep - i + ep_count) % ep_count
+        peer = place.partner(i)
         return remote(
             returned[c].at[0, peer], returned[c].at[1, peer], ss.at[c, i], sr.at[c, i],
             place.sibling(),
         )
 
-    for c, span in enumerate(r_spans):
-        value = jnp.dot(hidden, down_w[:, span], preferred_element_type=jnp.float32)
+    def down(c):
+        value = jnp.dot(hidden, down_w[:, r_spans[c]], preferred_element_type=jnp.float32)
         results[c][...] = value.astype(jnp.bfloat16).reshape(ep_count, capacity, -1)
         scatter(results[c], returned[c].at[0], c, bs, br)
         over(c, 0).start()
+
+    for c in range(min(LEAD, sent_back)):
+        down(c)
     s_hidden[...] = (
         (jax.nn.silu(s_gate_sum[...]) * s_up_sum[...])
         .astype(jnp.bfloat16)
@@ -458,14 +472,16 @@
 
     last = sent_back - 1
     for c in range(sent_back):
-        for i in range(1, ep_count):
+        if c > 0 and c + LEAD - 1 < sent_back:
+            down(c + LEAD - 1)
+        for i in place.turns():
             landing_wait(returned[c].at[0], c, i, bs, br)
             over(c, i).start()
         for i in range(ep_count):
-            peer = (place.ep - i + ep_count) % ep_count
+            peer = place.partner(i)
             block = returned[c].at[1, peer]
             remote(block, block, ss.at[c, i], sr.at[c, i], place.sibling()).wait_recv()
-        for d in range(chips - 1, 0 if c < last - 3 else 1, -1):
+        for d in range(chips - 1, 0 if c < PROMPT else 1, -1):
             from_edge(c, d)
         if c == 0:
             second.step(1, last=False, edge=False)
@@ -478,7 +494,7 @@
         if c > 1:
             from_middle(c - 2, 1)
     far_middle(last)
-    for c in range(max(0, last - 3), sent_back):
+    for c in range(PROMPT, sent_back):
         from_edge(c, 1)
     for c in range(max(0, last - 1), sent_back):
         from_middle(c, 1)
@@ -520,6 +536,8 @@
             pool_out, w_out[column // CORES, column % CORES], preferred_element_type=jnp.float32
         ).astype(jnp.bfloat16)
 
+    outs = [pltpu.make_async_copy(mixed, mixed_out, os.at[sent_back])]
+    outs[0].start()
     for c, span in enumerate(r_spans):
         for way in range(2):
 
@@ -528,8 +546,13 @@
 
             pl.when(place.behind(way, 1))(join)
         moe_out[:, span] = own[:, span].astype(jnp.bfloat16)
+        out = pltpu.make_async_copy(moe_out.at[:, span], moe_final.at[:, span], os.at[c])
+        out.start()
+        outs.append(out)
 
     halo.wait_send()
+    for out in outs:
+        out.wait()
     for copy in sent + shared:
         copy.wait_send()
     for c in range(sent_back):
@@ -541,6 +564,24 @@
             )
     for gather in gathers + [first, second]:
         gather.close()
+
+
+def settle_kernel(mixed, moe, mixed_out, moe_out, held, arrive, leave):
+    rows = mixed.shape[0] // CHUNKS
+    inward, outward = [], []
+    for n, (src, dst) in enumerate(((mixed, mixed_out), (moe, moe_out))):
+        for k in range(CHUNKS):
+            span = pl.ds(k * rows, rows)
+            block = held.at[n, span]
+            inward.append(pltpu.make_async_copy(src.at[span], block, arrive.at[n, k]))
+            outward.append(pltpu.make_async_copy(block, dst.at[span], leave.at[n, k]))
+    for copy in inward:
+        copy.start()
+    for n, copy in enumerate(inward):
+        copy.wait()
+        outward[n].start()
+    for copy in outward:
+        copy.wait()
 
 
 def shards(
@@ -597,6 +638,9 @@
             buffer(top_count, block_rows),
             pltpu.VMEM((1, width), f32),
             pltpu.VMEM((1, pool_scale.shape[0]), f32),
+            buffer(*mix_in.shape),
+            buffer(*moe_in.shape),
+            dma(1 + sent_back),
             dma(16),
             dma(gathered, 2 * messages + 1),
             dma(gathered, 2 * messages + 1),
@@ -616,17 +660,27 @@
             jax.ShapeDtypeStruct(moe_in.shape, bf16),
         ],
         in_specs=[pl.BlockSpec(memory_space=pltpu.HBM)] * 16,
-        out_specs=[pl.BlockSpec(memory_space=pltpu.VMEM)] * 2,
+        out_specs=[pl.BlockSpec(memory_space=pltpu.HBM)] * 2,
         scratch_shapes=scratch,
         compiler_params=pltpu.CompilerParams(
-            collective_id=0, has_side_effects=True, vmem_limit_bytes=67043328
+            collective_id=0, has_side_effects=True, vmem_limit_bytes=VMEM_BYTES
         ),
     )(
         moe_gain[None, :], routes.T, route_score.T, mix_gain[None, :], pool_scale[None, :],
         moe_in, pool_mat, shared_gate, shared_up, shared_down, mix_w_in, mix_w_out, mix_in,
         exp_gate, exp_up, exp_down,
     )
-    return (mixed, moe_out)
+    return pl.pallas_call(
+        settle_kernel,
+        out_shape=[
+            jax.ShapeDtypeStruct(mix_in.shape, bf16),
+            jax.ShapeDtypeStruct(moe_in.shape, bf16),
+        ],
+        in_specs=[pl.BlockSpec(memory_space=pltpu.HBM)] * 2,
+        out_specs=[pl.BlockSpec(memory_space=pltpu.HBM)] * 2,
+        scratch_shapes=[buffer(2, *mix_in.shape), dma(2, CHUNKS), dma(2, CHUNKS)],
+        compiler_params=pltpu.CompilerParams(vmem_limit_bytes=VMEM_BYTES),
+    )(mixed, moe_out)
 
 
 def solution(mesh):

time: 104 us -> 101 us (0.971)
  local copies, waits for them, and re-layouts: 3.76 us -> 0 us
    unnamed x2 -> x0, local copies, waits for them, and re-layouts: 3.76 us -> none
    pallas_call x0 -> x1, Pallas kernels: none -> 2.09 us  [shards(): pl.pallas_call(settle_kernel, out_shape=[jax.ShapeDtypeStruct(mix_in.shap...]
    pallas_call x1, Pallas kernels: 99.7 us -> 97.6 us  [shards(): pl.pallas_call(functools.partial(layer_kernel, ep_count, tp_count, seq_le...]
where the time goes in v3:
time: 101 us
  Pallas kernels  99.7 us (99%)
    pallas_call x1, Pallas kernels, shards(): pl.pallas_call(functools.partial(layer_kernel, ep_count, tp_count, seq_le...  97.6 us
    pallas_call x1, Pallas kernels, shards(): pl.pallas_call(settle_kernel, out_shape=[jax.ShapeDtypeStruct(mix_in.shap...  2.09 us

profile of v3, /device:TPU:0, one launch (start us, length us, event | category | flops | bytes accessed | tf_op | source)
XLA Modules:
  0.0 100.5 jit_solution(708338151983615689)
XLA Ops:
  0.6 97.6 %shard_map.167 = (bf16[128,2048]{1,0:T(8,128)(2,1)}, bf16[128,2048]{1,0:T(8,128)(2,1)}) custom-call(f32[1,2048]{1,0:T(1,128)} %bitcast.5, s32[2,1024]{1,0:T(2,128)} %bitcast.6, bf16[2,1024]{1,0:T(2,128)(2,1)} %bitcast.8, f32[1,2048]{1,0:T(1,128)} %bitcast.7, f32[1,512]{1,0:T(1,128)} %bitcast.9, bf16[128,2048]{1,0:T(8,128)(2,1)} %moe_in.1, ...), custom_call_target="tpu_custom_call" | custom-call | tf_op jit(solution)/shard_map/pallas_call | solution.py:656
  98.3 2.1 %shard_map.168 = (bf16[128,2048]{1,0:T(8,128)(2,1)}, bf16[128,2048]{1,0:T(8,128)(2,1)}) custom-call(bf16[128,2048]{1,0:T(8,128)(2,1)} %get-tuple-element.4.mixed, bf16[128,2048]{1,0:T(8,128)(2,1)} %get-tuple-element.5.moe), custom_call_target="tpu_custom_call" | custom-call | tf_op jit(solution)/shard_map/pallas_call | solution.py:673

commit v4 on v3

--- a/solution.py
+++ b/solution.py
@@ -18,7 +18,7 @@
 PROMPT = 2
 VMEM_BYTES = 67043328
 CHUNKS = 4
-GATHER_CUTS = (1, 1, 1, 1, 1, 1, 1, 1)
+GATHER_CUTS = (1, 2, 2, 2, 2, 2, 2, 2, 1)
 RETURN_CUTS = (1, 1, 2, 2, 2, 2, 2, 2, 2)
 
 
@@ -323,6 +323,17 @@
             value = jnp.dot(block, weights[span, :], preferred_element_type=jnp.float32)
             acc_ref[...] = value if c == 0 else acc_ref[...] + value
 
+    def products_of_shared():
+        for acc_ref, part in ((s_gate_sum, s_gate), (s_up_sum, s_up)):
+            value = 0.0
+            for c, span in enumerate(g_spans):
+                value = value + lax.dot_general(
+                    tokens[c][:, pl.ds(core, 1)].reshape(chips * rows, -1),
+                    part[:, :, span].reshape(-1, span.stop - span.start), across,
+                    preferred_element_type=jnp.float32,
+                )
+            acc_ref[...] = value
+
     lag = 3
     for turn in range(gathered + chips - 2):
         for d in range(1, chips):
@@ -372,18 +383,10 @@
     )
     halo.start()
 
-    for c in range(gathered - lag, gathered - 1):
+    for c in range(gathered - lag, gathered):
+        if c == gathered - 2:
+            products_of_shared()
         gate_up(c)
-    for acc_ref, part in ((s_gate_sum, s_gate), (s_up_sum, s_up)):
-        value = 0.0
-        for c, span in enumerate(g_spans):
-            value = value + lax.dot_general(
-                tokens[c][:, pl.ds(core, 1)].reshape(chips * rows, -1),
-                part[:, :, span].reshape(-1, span.stop - span.start), across,
-                preferred_element_type=jnp.float32,
-            )
-        acc_ref[...] = value
-    gate_up(gathered - 1)
     hidden = (jax.nn.silu(gate_sum[...]) * up_sum[...]).astype(jnp.bfloat16)
 
     def over(c, i):

time: 101 us -> 101 us (level)
  no operation moved by 1% of the time
where the time goes in v4:
time: 101 us; the launch traced here: 100 us
  Pallas kernels  99.4 us (98%)
    pallas_call x1, Pallas kernels, shards(): pl.pallas_call(functools.partial(layer_kernel, ep_count, tp_count, seq_le...  97.3 us
    pallas_call x1, Pallas kernels, shards(): pl.pallas_call(settle_kernel, out_shape=[jax.ShapeDtypeStruct(mix_in.shap...  2.09 us

profile of v4, /device:TPU:0, one launch (start us, length us, event | category | flops | bytes accessed | tf_op | source)
XLA Modules:
  0.0 100.3 jit_solution(10088418763943380650)
XLA Ops:
  0.6 97.3 %shard_map.167 = (bf16[128,2048]{1,0:T(8,128)(2,1)}, bf16[128,2048]{1,0:T(8,128)(2,1)}) custom-call(f32[1,2048]{1,0:T(1,128)} %bitcast.5, s32[2,1024]{1,0:T(2,128)} %bitcast.6, bf16[2,1024]{1,0:T(2,128)(2,1)} %bitcast.8, f32[1,2048]{1,0:T(1,128)} %bitcast.7, f32[1,512]{1,0:T(1,128)} %bitcast.9, bf16[128,2048]{1,0:T(8,128)(2,1)} %moe_in.1, ...), custom_call_target="tpu_custom_call" | custom-call | tf_op jit(solution)/shard_map/pallas_call | solution.py:659
  98.0 2.1 %shard_map.168 = (bf16[128,2048]{1,0:T(8,128)(2,1)}, bf16[128,2048]{1,0:T(8,128)(2,1)}) custom-call(bf16[128,2048]{1,0:T(8,128)(2,1)} %get-tuple-element.4.mixed, bf16[128,2048]{1,0:T(8,128)(2,1)} %get-tuple-element.5.moe), custom_call_target="tpu_custom_call" | custom-call | tf_op jit(solution)/shard_map/pallas_call | solution.py:676
